TPU v7x, 32 devices: a whole 2x2x4 slice. The times are simulated.
32 devices in a mesh: sp: 8 (over z, y), tp: 4 (over x, core).
Axes of the slice: x: 2, y: 2, z: 4, core: 2. Of those that a mesh axis runs over, the one named last changes fastest.
Arguments:
- stream: bfloat16 [8192, 2048], P(('sp', 'tp')), may hold values from -6 to 6
- query_rows: bfloat16 [8192, 1024], P('sp', 'tp'), may hold values from -6 to 6
- key_rows: bfloat16 [8192, 1024], P('sp', 'tp'), may hold values from -6 to 6
- value_rows: bfloat16 [8192, 2048], P('sp', 'tp'), may hold values from -6 to 6
- gate_rows: bfloat16 [8192, 2048], P('sp', 'tp'), may hold values from -6 to 6
- log_decay: float32 [8192, 1024], P('sp', 'tp'), may hold values from -1 to 0
- head_gain: float32 [256], replicated, may hold values from 0.1 to 1.9
- out_weight: bfloat16 [2048, 2048], P('tp'), may hold values from -0.125 to 0.125
- mix_gain: float32 [2048], replicated, may hold values from 0.1 to 1.9
- up_weight: bfloat16 [2048, 8192], P('sp', 'tp'), may hold values from -0.125 to 0.125
- down_weight: bfloat16 [2048, 8192], P('sp', 'tp'), may hold values from -0.0625 to 0.0625
Outputs:
- mixed_out: bfloat16 [8192, 2048], P(('sp', 'tp'))
All inputs are finite; a program needn't handle non-finite values.
Results may differ from a plain program's by a relative error of at most 0.02.
Values may be sent and summed in bfloat16 or wider, within the bound.
A program may use at most 128 MiB of HBM per device.

v0:
```python
import jax
import jax.numpy as jnp
from jax import lax
from jax.sharding import PartitionSpec as P

KEY_CHANNELS = 128
DV = 256
BLOCK = 64
EPS = 1e-06


def prefix(shard, axis, join, neutral):
    place = lax.axis_index(axis)
    gathered = jax.tree.map(
        lambda a, kind: lax.all_gather(a.astype(kind), axis), shard, (jnp.bfloat16, jnp.bfloat16)
    )
    state = jax.tree.map(lambda a, e: jnp.zeros_like(a) + jnp.asarray(e, a.dtype), shard, neutral)

    def one(step, state):
        return join(
            state,
            jax.tree.map(
                lambda a, own: lax.dynamic_index_in_dim(a, step, 0, False).astype(own.dtype),
                gathered,
                shard,
            ),
        )

    return lax.fori_loop(0, place, one, state)


def chain(earlier, later):
    return (earlier[0] * later[0], later[0][..., None] * earlier[1] + later[1])


def squared_relu(pre):
    return jnp.square(jax.nn.relu(pre)).astype(jnp.bfloat16)


def local(
    stream,
    query_rows,
    key_rows,
    value_rows,
    gate_rows,
    log_decay,
    head_gain,
    out_weight,
    mix_gain,
    up_weight,
    down_weight,
):
    rows = query_rows.shape[0]
    heads_here = query_rows.shape[1] // KEY_CHANNELS
    count = rows // BLOCK
    queries = query_rows.astype(jnp.float32).reshape(
        count, BLOCK, heads_here, KEY_CHANNELS
    ) * KEY_CHANNELS ** (-0.5)
    keys_all = key_rows.astype(jnp.float32).reshape(count, BLOCK, heads_here, KEY_CHANNELS)
    values_all = value_rows.astype(jnp.float32).reshape(count, BLOCK, heads_here, DV)
    decay_rates = log_decay.reshape(count, BLOCK, heads_here, KEY_CHANNELS)
    cum = jnp.cumsum(decay_rates, axis=1)
    last = cum[:, -1:]
    decayed_state = keys_all * jnp.exp(last - cum)
    state_updates = jnp.einsum(
        "nshk,nshv->nhkv", decayed_state, values_all, precision=lax.Precision.HIGHEST
    )
    end_log = last[:, 0]
    total_log = jnp.cumsum(end_log, axis=0)
    tail_weights = jnp.exp(total_log[-1] - total_log)
    summary_state = jnp.einsum(
        "mfa,mfaq->faq", tail_weights, state_updates, precision=lax.Precision.HIGHEST
    )
    summary_decay = jnp.exp(total_log[-1])
    incoming = prefix(
        (summary_decay, summary_state),
        "sp",
        chain,
        (jnp.ones_like(summary_decay), jnp.zeros_like(summary_state)),
    )

    def step(matrix_state, inputs):
        factor, state_update, query_block = inputs
        matrix_state = factor[..., None] * matrix_state + state_update
        head_output = jnp.einsum(
            "wle,leg->wlg", query_block, matrix_state, precision=lax.Precision.HIGHEST
        )
        return (matrix_state, head_output)

    _, outs = lax.scan(step, incoming[1], (jnp.exp(end_log), state_updates, queries))
    readout = outs.reshape(rows, heads_here, DV)
    scaled = readout * lax.rsqrt(jnp.mean(readout * readout, axis=-1, keepdims=True) + EPS)
    gates = gate_rows.astype(jnp.float32).reshape(rows, heads_here, DV)
    gated = scaled * head_gain * jax.nn.silu(gates)
    heads_out = gated.reshape(rows, heads_here * DV).astype(jnp.bfloat16)
    whole_weight = lax.all_gather(out_weight, "tp", axis=0, tiled=True)
    mine = lax.all_to_all(heads_out, "tp", split_axis=0, concat_axis=1, tiled=True)
    attn = jnp.dot(mine, whole_weight, preferred_element_type=jnp.float32)
    midf = (stream.astype(jnp.float32) + attn).astype(jnp.bfloat16).astype(jnp.float32)
    normed = (
        midf * lax.rsqrt(jnp.mean(midf * midf, axis=-1, keepdims=True) + EPS) * mix_gain
    ).astype(jnp.bfloat16)
    gathered = lax.all_gather(normed, "tp", axis=0, tiled=True)
    pre = jnp.dot(
        gathered,
        lax.all_gather(up_weight, "sp", axis=0, tiled=True),
        preferred_element_type=jnp.float32,
    )
    hidden = squared_relu(pre)
    down_full = lax.all_gather(down_weight, "sp", axis=0, tiled=True)
    feed = lax.psum_scatter(
        lax.dot_general(
            hidden, down_full, (((1,), (1,)), ((), ())), preferred_element_type=jnp.float32
        ).astype(jnp.bfloat16),
        "tp",
        scatter_dimension=0,
        tiled=True,
    ).astype(jnp.float32)
    return (midf + feed).astype(jnp.bfloat16)


def solution(mesh):
    placed = (
        P(("sp", "tp"), None),
        P("sp", "tp"),
        P("sp", "tp"),
        P("sp", "tp"),
        P("sp", "tp"),
        P("sp", "tp"),
        P(),
        P("tp", None),
        P(),
        P("sp", "tp"),
        P("sp", "tp"),
    )
    return jax.shard_map(
        local, mesh=mesh, in_specs=placed, out_specs=P(("sp", "tp"), None), check_vma=False
    )
```

profile of v0, /device:TPU:0, one launch (start us, length us, event | category | flops | bytes accessed | tf_op | source)
XLA Modules:
  0.0 489.8 jit_solution(16888176910479370243)
XLA Ops:
  6.5 1.8 reshape.64
  9.1 1.6 reshape.72
  11.4 1.3 reshape.67
  12.7 2.0 fusion.13
  14.8 4.6 fusion.1
  22.2 22.3 %all_gather.22 = bf16[8,2,128]{2,1,0:T(2,128)(2,1)S(1)} all-gather(bf16[1,2,128]{2,1,0:T(2,128)(2,1)S(1)} %get-tuple-element.136), channel_id=1, replica_groups=mesh['sp'=8,'tp'=4] {'sp'}, dimensions={0}, use_global_device_ids=true | all-gather | bytes 4608 | tf_op jit(solution)/shard_map/all_gather | solution.py:15
  44.5 1.1 convert_multiply_fusion.3
  45.6 1.5 mul.94
  47.1 16.1 %all-gather.15.cloned.1.call-done = bf16[16,128,256]{2,1,0:T(8,128)(2,1)} async-done(((bf16[2,128,256]{2,1,0:T(8,128)(2,1)}), bf16[16,128,256]{2,1,0:T(8,128)(2,1)}) %all-gather.15.cloned.1.call-update) | async-done | bytes 1048592 | tf_op jit(solution)/shard_map/all_gather | solution.py:15
  63.4 36.3 %while.25 = (s32[]{:T(128)}, f32[2,128,256]{2,1,0:T(8,128)S(1)}, f32[16,64,2,256]{3,1,2,0:T(8,128)S(1)}, f32[16,2,128]{2,0,1:T(8,128)S(1)}, f32[16,2,128,256]{3,...) while((s32[]{:T(128)}, f32[2,128,256]{2,1,0:T(8,128)S(1)}, f32[16,64,2,256]{3,1,2,0:T(8,128)S(1)}, ...), condition=%wide.region_5.6_spmd, body=%wide.region_4.5_spmd.sunk | while | flops 50462720 | bytes 1379421 | solution.py:90
  70.2 1.1 bitcast_add_fusion.2
  72.6 1.1 bitcast_add_fusion.2
  99.7 3.0 copy.53
  103.4 1.2 mul.96
  104.8 1.4 copy-done.3
  108.7 22.5 %all_to_all.19 = bf16[4,256,512]{1,2,0:T(8,128)(2,1)S(1)} all-to-all(bf16[4,256,512]{1,2,0:T(8,128)(2,1)S(1)} %copy.56), channel_id=1, replica_groups=mesh['sp'=8,'tp'=4] {'tp'}, dimensions={0} | all-to-all | bytes 2097152 | tf_op jit(solution)/shard_map/all_to_all | solution.py:97
  131.2 6.5 %fusion.8 = (f32[256]{0:T(256)S(1)}, bf16[256,2048]{1,0:T(8,128)(2,1)S(1)}) fusion(bf16[256,2048]{0,1:T(8,128)(2,1)S(1)} %bitcast.70, bf16[2048,2048]{1,0:T(8,128)(2,1)} %all-gather.7.cloned.1.call-done, bf16[256,2048]{1,0:T(8,128)(2,1)} %param.15), kind=kOutput, calls=%fused_computation.23 | convolution fusion | flops 2150629120 | bytes 11535360 | tf_op jit(solution)/shard_map/dot_general | solution.py:98
  137.7 1.3 fusion.10
  139.3 112.1 %all-gather.11.cloned.1.call-done = bf16[2048,2048]{1,0:T(8,128)(2,1)} async-done(((bf16[256,2048]{1,0:T(8,128)(2,1)}), bf16[2048,2048]{1,0:T(8,128)(2,1)}) %all-gather.11.cloned.1.call-update) | async-done | bytes 8388624 | tf_op jit(solution)/shard_map/all_gather | solution.py:106
  251.4 124.7 %all-gather.13.cloned.1.call-done = bf16[2048,2048]{1,0:T(8,128)(2,1)} async-done(((bf16[256,2048]{1,0:T(8,128)(2,1)}), bf16[2048,2048]{1,0:T(8,128)(2,1)}) %all-gather.13.cloned.1.call-update) | async-done | bytes 8388624 | tf_op jit(solution)/shard_map/all_gather | solution.py:110
  376.1 34.1 %all-gather.9.cloned.1.call-done = bf16[1024,2048]{1,0:T(8,128)(2,1)} async-done(((bf16[256,2048]{1,0:T(8,128)(2,1)}), bf16[1024,2048]{1,0:T(8,128)(2,1)}) %all-gather.9.cloned.1.call-update) | async-done | bytes 4194320 | tf_op jit(solution)/shard_map/all_gather | solution.py:103
  410.2 25.4 %convolution_convert_fusion = bf16[1024,2048]{1,0:T(8,128)(2,1)} fusion(bf16[2048,2048]{1,0:T(8,128)(2,1)} %all-gather.13.cloned.1.call-done, bf16[1024,2048]{1,0:T(8,128)(2,1)} %all-gather.9.cloned.1.call-done, bf16[2048,2048]{1,0:T(8,128)(2,1)} %all-gather.11.cloned.1.call-done), kind=kOutput, calls=%fused_computation.11 | convolution fusion | flops 17188257792 | bytes 25165824 | tf_op jit(solution)/shard_map/dot_general | solution.py:112
  435.6 44.7 %reduce-scatter.2.cloned.1.call-done = bf16[256,2048]{1,0:T(8,128)(2,1)} async-done(((bf16[1024,2048]{1,0:T(8,128)(2,1)}), bf16[256,2048]{1,0:T(8,128)(2,1)}) %reduce-scatter.2.cloned.1.call-update) | async-done | bytes 1048592 | tf_op jit(solution)/shard_map/reduce_scatter | solution.py:111
  480.3 2.6 fusion.11
  (108 shorter events, 41.5 us)
Async XLA Ops:
  6.5 40.6 %copy-start = (f32[256]{0:T(256)S(1)}, f32[256]{0:T(256)}, u32[]{:S(2)}) copy-start(f32[256]{0:T(256)} %param.21) | copy-start | bytes 3076
  6.5 56.7 %all-gather.15.cloned.1.call-start = ((), (), s32[]{:S(2)}) async-start(), calls=%async_computation.7 | async-start | bytes 1179648 | tf_op jit(solution)/shard_map/all_gather | solution.py:15
  14.7 4.6 copy-start.2
  20.1 111.2 %all-gather.7.cloned.1.call-start = ((), (), s32[]{:S(2)}) async-start(), calls=%async_computation.2 | async-start | bytes 10485760 | tf_op jit(solution)/shard_map/all_gather | solution.py:96
  20.8 230.6 %all-gather.11.cloned.1.call-start = ((), (), s32[]{:S(2)}) async-start(), calls=%async_computation.4 | async-start | bytes 9437184 | tf_op jit(solution)/shard_map/all_gather | solution.py:106
  21.5 354.6 %all-gather.13.cloned.1.call-start = ((), (), s32[]{:S(2)}) async-start(), calls=%async_computation.5 | async-start | bytes 9437184 | tf_op jit(solution)/shard_map/all_gather | solution.py:110
  22.1 388.1 %all-gather.9.cloned.1.call-start = ((), (), s32[]{:S(2)}) async-start(), calls=%async_computation.3 | async-start | bytes 5242880 | tf_op jit(solution)/shard_map/all_gather | solution.py:103
  104.6 1.6 copy-start.3
  106.2 1.2 copy-start.4
  131.2 6.5 %copy-start.5 = (f32[2048]{0:T(1024)S(1)}, f32[2048]{0:T(1024)}, u32[]{:S(2)}) copy-start(f32[2048]{0:T(1024)} %param.23) | copy-start | bytes 24580
  139.0 341.3 %reduce-scatter.2.cloned.1.call-start = ((), (), s32[]{:S(2)}) async-start(), calls=%async_computation.6 | async-start | bytes 5242880 | tf_op jit(solution)/shard_map/reduce_scatter | solution.py:111
  435.6 47.3 %copy-start.1 = (f32[256]{0:T(256)S(1)}, f32[256]{0:T(256)}, u32[]{:S(2)}) copy-start(f32[256]{0:T(256)} %param.21) | copy-start | bytes 3076
Sparse Core Ops, SparseCore 0:
  20.2 42.9 all-gather.14
  64.8 62.6 all-gather.6
  129.6 121.8 all-gather.10
  253.4 122.6 all-gather.12
  377.5 32.6 all-gather.8
  435.7 44.5 reduce-scatter.1
where the time goes:
time: 492 us; the launch traced here: 490 us
  waiting for transfers between devices  334 us (68%)
  blocking collectives  44.8 us (9%)
  matrix products  43.1 us (9%)
  local copies, waits for them, and re-layouts  28.6 us (6%)
  other arithmetic  24.7 us (5%)
  between operations  13.7 us (3%)
    all_gather x1, waiting for transfers between devices, local(): down_full = lax.all_gather(down_weight, 'sp', axis=0, tiled=True)  125 us
    all_gather x1, waiting for transfers between devices, local(): lax.all_gather(up_weight, 'sp', axis=0, tiled=True)  112 us
    reduce_scatter x1, waiting for transfers between devices, local(): lax.psum_scatter(lax.dot_general(hidden, down_full, (((1,), (1,)), ((), (...  44.7 us
    all_gather x1, waiting for transfers between devices, local(): gathered = lax.all_gather(normed, 'tp', axis=0, tiled=True)  34.1 us
    dot_general x1, matrix products, local(): lax.dot_general(hidden, down_full, (((1,), (1,)), ((), ())), preferred_el...  25.4 us
    all_to_all x1, blocking collectives, local(): lax.all_to_all(heads_out, 'tp', split_axis=0, concat_axis=1, tiled=True)  22.5 us
    all_gather x1, blocking collectives, prefix(): lax.all_gather(a.astype(kind), axis)  22.3 us
    add x16, other arithmetic, step(): matrix_state = factor[..., None] * matrix_state + state_update  17.2 us
  transfers between devices with their start and end apart: 6, of which 5 were waited for; matrix products, arithmetic and copies ran while one was open for 11% of the time, Pallas kernels for 0%

commit v1 on v0

--- a/solution.py
+++ b/solution.py
@@ -100,7 +100,12 @@
     normed = (
         midf * lax.rsqrt(jnp.mean(midf * midf, axis=-1, keepdims=True) + EPS) * mix_gain
     ).astype(jnp.bfloat16)
-    gathered = lax.all_gather(normed, "tp", axis=0, tiled=True)
+    ring = [normed]
+    for hop in range(3):
+        ring.append(lax.ppermute(ring[-1], "tp", [(dev, (dev + 1) % 4) for dev in range(4)]))
+    gathered = jnp.roll(
+        jnp.concatenate(ring[::-1], axis=0), (lax.axis_index("tp") + 1) * ring[0].shape[0], axis=0
+    )
     pre = jnp.dot(
         gathered,
         lax.all_gather(up_weight, "sp", axis=0, tiled=True),

time: 492 us -> 459 us (0.933)
  waiting for transfers between devices: 334 us -> 289 us
  local copies, waits for them, and re-layouts: 28.6 us -> 37.9 us
    all_gather x1, waiting for transfers between devices: 125 us -> 60.9 us  [local(): down_full = lax.all_gather(down_weight, 'sp', axis=0, tiled=True)]
    ppermute x0 -> x3, waiting for transfers between devices: none -> 42.8 us  [local(): lax.ppermute(ring[-1], 'tp', [(dev, (dev + 1) % 4) for dev in range(4)])]
    all_gather x1 -> x0, waiting for transfers between devices: 34.1 us -> none  [local(): gathered = lax.all_gather(normed, 'tp', axis=0, tiled=True)]
    all_gather x1, waiting for transfers between devices: 112 us -> 125 us  [local(): lax.all_gather(up_weight, 'sp', axis=0, tiled=True)]
    unnamed x16 -> x22, local copies, waits for them, and re-layouts: 2.82 us -> 12.2 us
  transfers between devices with their start and end apart: 6 -> 8, of which waited for: 5 -> 7; matrix products, arithmetic and copies ran while one was open for 11% -> 14% of each run, Pallas kernels for 0% -> 0%
where the time goes in v1:
time: 459 us; the launch traced here: 457 us
  waiting for transfers between devices  289 us (63%)
  blocking collectives  46.4 us (10%)
  matrix products  42.7 us (9%)
  local copies, waits for them, and re-layouts  37.9 us (8%)
  other arithmetic  26.4 us (6%)
  between operations  13.4 us (3%)
    all_gather x1, waiting for transfers between devices, local(): lax.all_gather(up_weight, 'sp', axis=0, tiled=True)  125 us
    all_gather x1, waiting for transfers between devices, local(): down_full = lax.all_gather(down_weight, 'sp', axis=0, tiled=True)  60.9 us
    reduce_scatter x1, waiting for transfers between devices, local(): lax.psum_scatter(lax.dot_general(hidden, down_full, (((1,), (1,)), ((), (...  42.9 us
    ppermute x3, waiting for transfers between devices, local(): lax.ppermute(ring[-1], 'tp', [(dev, (dev + 1) % 4) for dev in range(4)])  42.8 us
    dot_general x1, matrix products, local(): lax.dot_general(hidden, down_full, (((1,), (1,)), ((), ())), preferred_el...  25.4 us
    all_to_all x1, blocking collectives, local(): lax.all_to_all(heads_out, 'tp', split_axis=0, concat_axis=1, tiled=True)  24.1 us
    all_gather x1, blocking collectives, prefix(): lax.all_gather(a.astype(kind), axis)  22.3 us
    add x16, other arithmetic, step(): matrix_state = factor[..., None] * matrix_state + state_update  17.2 us
  transfers between devices with their start and end apart: 8, of which 7 were waited for; matrix products, arithmetic and copies ran while one was open for 14% of the time, Pallas kernels for 0%

profile of v1, /device:TPU:0, one launch (start us, length us, event | category | flops | bytes accessed | tf_op | source)
XLA Modules:
  0.0 457.1 jit_solution(16293838050907203109)
XLA Ops:
  6.5 1.8 reshape.64
  9.1 1.6 reshape.72
  11.4 1.3 reshape.67
  12.7 2.0 fusion.20
  14.8 2.0 copy-done.2
  16.7 4.6 %fusion.1 = bf16[2,128,1,256]{3,2,1,0:T(2,128)(2,1)S(1)} fusion(f32[16,2,128,1]{0,3,2,1:T(1,128)S(1)} %copy.57, f32[16,2,128,256]{3,2,1,0:T(8,128)S(1)} %fusion.20), kind=kOutput, calls=%fused_computation.9 | convolution fusion | flops 12582912 | bytes 4341760 | tf_op jit(solution)/shard_map/mfa,mfaq->faq/dot_general | solution.py:71
  24.1 22.3 %all_gather.19 = bf16[8,2,128]{2,1,0:T(2,128)(2,1)S(1)} all-gather(bf16[1,2,128]{2,1,0:T(2,128)(2,1)S(1)} %get-tuple-element.136), channel_id=1, replica_groups=mesh['sp'=8,'tp'=4] {'sp'}, dimensions={0}, use_global_device_ids=true | all-gather | bytes 4608 | tf_op jit(solution)/shard_map/all_gather | solution.py:15
  47.6 1.5 mul.97
  49.1 16.1 %all-gather.12.cloned.1.call-done = bf16[16,128,256]{2,1,0:T(8,128)(2,1)} async-done(((bf16[2,128,256]{2,1,0:T(8,128)(2,1)}), bf16[16,128,256]{2,1,0:T(8,128)(2,1)}) %all-gather.12.cloned.1.call-update) | async-done | bytes 1048592 | tf_op jit(solution)/shard_map/all_gather | solution.py:15
  65.4 36.2 %while.25 = (s32[]{:T(128)}, f32[2,128,256]{2,1,0:T(8,128)S(1)}, f32[16,64,2,256]{3,1,2,0:T(8,128)S(1)}, f32[16,2,128]{2,0,1:T(8,128)S(1)}, f32[16,2,128,256]{3,...) while((s32[]{:T(128)}, f32[2,128,256]{2,1,0:T(8,128)S(1)}, f32[16,64,2,256]{3,1,2,0:T(8,128)S(1)}, ...), condition=%wide.region_5.6_spmd, body=%wide.region_4.5_spmd.sunk | while | flops 50462720 | bytes 1379421 | solution.py:90
  101.6 3.0 copy.53
  109.1 24.1 %all_to_all.19 = bf16[4,256,512]{1,2,0:T(8,128)(2,1)S(1)} all-to-all(bf16[4,256,512]{1,2,0:T(8,128)(2,1)S(1)} %copy.56), channel_id=1, replica_groups=mesh['sp'=8,'tp'=4] {'tp'}, dimensions={0} | all-to-all | bytes 2097152 | tf_op jit(solution)/shard_map/all_to_all | solution.py:97
  133.2 6.1 %fusion.15 = (f32[256]{0:T(256)S(1)}, bf16[256,2048]{1,0:T(8,128)(2,1)S(1)}) fusion(bf16[256,2048]{0,1:T(8,128)(2,1)S(1)} %bitcast.69, bf16[2048,2048]{1,0:T(8,128)(2,1)} %all-gather.6.cloned.1.call-done, bf16[256,2048]{1,0:T(8,128)(2,1)} %param.15), kind=kOutput, calls=%fused_computation.25 | convolution fusion | flops 2150629120 | bytes 11535360 | tf_op jit(solution)/shard_map/dot_general | solution.py:98
  139.7 14.2 %collective-permute-done = bf16[256,2048]{1,0:T(8,128)(2,1)S(1)} collective-permute-done((bf16[256,2048]{1,0:T(8,128)(2,1)S(1)}, bf16[256,2048]{1,0:T(8,128)(2,1)S(1)}, u32[]{:S(2)}, u32[]{:S(2)}) %collective-permute-start) | collective-permute-done | bytes 1048608 | tf_op jit(solution)/shard_map/ppermute | solution.py:105
  153.9 14.2 %collective-permute-done.1 = bf16[256,2048]{1,0:T(8,128)(2,1)S(1)} collective-permute-done((bf16[256,2048]{1,0:T(8,128)(2,1)S(1)}, bf16[256,2048]{1,0:T(8,128)(2,1)S(1)}, u32[]{:S(2)}, u32[]{:S(2)}) %collective-permute-start.1) | collective-permute-done | bytes 1048608 | tf_op jit(solution)/shard_map/ppermute | solution.py:105
  168.1 14.3 %collective-permute-done.2 = bf16[256,2048]{1,0:T(8,128)(2,1)} collective-permute-done((bf16[256,2048]{1,0:T(8,128)(2,1)S(1)}, bf16[256,2048]{1,0:T(8,128)(2,1)}, u32[]{:S(2)}, u32[]{:S(2)}) %collective-permute-start.2) | collective-permute-done | bytes 1048608 | tf_op jit(solution)/shard_map/ppermute | solution.py:105
  182.5 2.4 constant_dynamic-update-slice_fusion.7
  188.3 2.3 constant_dynamic-update-slice_fusion.3
  192.7 1.3 constant_dynamic-update-slice_fusion
  194.0 60.9 %all-gather.10.cloned.1.call-done = bf16[2048,2048]{1,0:T(8,128)(2,1)} async-done(((bf16[256,2048]{1,0:T(8,128)(2,1)}), bf16[2048,2048]{1,0:T(8,128)(2,1)}) %all-gather.10.cloned.1.call-update) | async-done | bytes 8388624 | tf_op jit(solution)/shard_map/all_gather | solution.py:115
  255.0 124.7 %all-gather.8.cloned.1.call-done = bf16[2048,2048]{1,0:T(8,128)(2,1)} async-done(((bf16[256,2048]{1,0:T(8,128)(2,1)}), bf16[2048,2048]{1,0:T(8,128)(2,1)}) %all-gather.8.cloned.1.call-update) | async-done | bytes 8388624 | tf_op jit(solution)/shard_map/all_gather | solution.py:111
  379.6 25.4 %fusion.7 = bf16[1024,2048]{1,0:T(8,128)(2,1)} fusion(bf16[2048,2048]{1,0:T(8,128)(2,1)} %all-gather.10.cloned.1.call-done, bf16[2048,2048]{1,0:T(8,128)(2,1)} %all-gather.8.cloned.1.call-done, bf16[2048,2048]{1,0:T(8,128)(2,1)} %constant_dynamic-update-slice_fusion, s32[]{:T(128)S(6)} %select_n.21), kind=kOutput, calls=%fused_computation.13 | convolution fusion | flops 17188257792 | bytes 25165828 | tf_op jit(solution)/shard_map/dot_general | solution.py:117
  405.1 42.9 %reduce-scatter.2.cloned.1.call-done = bf16[256,2048]{1,0:T(8,128)(2,1)} async-done(((bf16[1024,2048]{1,0:T(8,128)(2,1)}), bf16[256,2048]{1,0:T(8,128)(2,1)}) %reduce-scatter.2.cloned.1.call-update) | async-done | bytes 1048592 | tf_op jit(solution)/shard_map/reduce_scatter | solution.py:116
  448.0 2.6 fusion.18
  (119 shorter events, 51.5 us)
Async XLA Ops:
  6.5 42.5 %copy-start = (f32[256]{0:T(256)S(1)}, f32[256]{0:T(256)}, u32[]{:S(2)}) copy-start(f32[256]{0:T(256)} %param.21) | copy-start | bytes 3076
  6.5 58.6 %all-gather.12.cloned.1.call-start = ((), (), s32[]{:S(2)}) async-start(), calls=%async_computation.6 | async-start | bytes 1179648 | tf_op jit(solution)/shard_map/all_gather | solution.py:15
  14.7 2.0 copy-start.2
  22.0 111.2 %all-gather.6.cloned.1.call-start = ((), (), s32[]{:S(2)}) async-start(), calls=%async_computation.2 | async-start | bytes 10485760 | tf_op jit(solution)/shard_map/all_gather | solution.py:96
  22.8 232.2 %all-gather.10.cloned.1.call-start = ((), (), s32[]{:S(2)}) async-start(), calls=%async_computation.4 | async-start | bytes 9437184 | tf_op jit(solution)/shard_map/all_gather | solution.py:115
  23.5 356.1 %all-gather.8.cloned.1.call-start = ((), (), s32[]{:S(2)}) async-start(), calls=%async_computation.3 | async-start | bytes 9437184 | tf_op jit(solution)/shard_map/all_gather | solution.py:111
  24.1 423.9 %reduce-scatter.2.cloned.1.call-start = ((), (), s32[]{:S(2)}) async-start(), calls=%async_computation.5 | async-start | bytes 5242880 | tf_op jit(solution)/shard_map/reduce_scatter | solution.py:116
  105.0 1.7 copy-start.3
  106.5 1.2 copy-start.4
  133.2 6.1 %copy-start.5 = (f32[2048]{0:T(1024)S(1)}, f32[2048]{0:T(1024)}, u32[]{:S(2)}) copy-start(f32[2048]{0:T(1024)} %param.23) | copy-start | bytes 24580
  139.6 14.3 %collective-permute-start = (bf16[256,2048]{1,0:T(8,128)(2,1)S(1)}, bf16[256,2048]{1,0:T(8,128)(2,1)S(1)}, u32[]{:S(2)}, u32[]{:S(2)}) collective-permute-start(bf16[256,2048]{1,0:T(8,128)(2,1)S(1)} %fusion.17), channel_id=1, source_target_pairs={{0,1},{1,2},{2,3},{3,0},{4,5},{5,6},{6,7},{7,4},{8,9},{9,10},{10,1... | collective-permute-start | bytes 3145736 | tf_op jit(solution)/shard_map/ppermute | solution.py:105
  153.9 14.2 %collective-permute-start.1 = (bf16[256,2048]{1,0:T(8,128)(2,1)S(1)}, bf16[256,2048]{1,0:T(8,128)(2,1)S(1)}, u32[]{:S(2)}, u32[]{:S(2)}) collective-permute-start(bf16[256,2048]{1,0:T(8,128)(2,1)S(1)} %collective-permute-done), channel_id=1, source_target_pairs={{0,1},{1,2},{2,3},{3,0},{4,5},{5,6},{6,7},{7,4},{8,9},{9,10},{10,1... | collective-permute-start | bytes 3145736 | tf_op jit(solution)/shard_map/ppermute | solution.py:105
  168.1 14.3 %collective-permute-start.2 = (bf16[256,2048]{1,0:T(8,128)(2,1)S(1)}, bf16[256,2048]{1,0:T(8,128)(2,1)}, u32[]{:S(2)}, u32[]{:S(2)}) collective-permute-start(bf16[256,2048]{1,0:T(8,128)(2,1)S(1)} %collective-permute-done.1), channel_id=1, source_target_pairs={{0,1},{1,2},{2,3},{3,0},{4,5},{5,6},{6,7},{7,4},{8,9},{9,10},{10,1... | collective-permute-start | bytes 3145736 | tf_op jit(solution)/shard_map/ppermute | solution.py:105
  379.6 70.9 %copy-start.1 = (f32[256]{0:T(256)S(1)}, f32[256]{0:T(256)}, u32[]{:S(2)}) copy-start(f32[256]{0:T(256)} %param.21) | copy-start | bytes 3076
Sparse Core Ops, SparseCore 0:
  22.1 42.9 all-gather.11
  66.7 64.1 all-gather.5
  133.1 121.8 all-gather.9
  256.9 122.6 all-gather.7
  405.2 42.7 reduce-scatter.1
